TPU v7x, 512 devices: a 4x2x32 block of a 4x8x32 slice. The times are simulated.
512 devices in a mesh: grp: 2 (over y), fs: 32 (over z), tp: 8 (over x, core).
Axes of the slice: x: 4, y: 2, z: 32, core: 2. Of those that a mesh axis runs over, the one named last changes fastest.
The devices are a block of a 4x8x32 slice.
Arguments:
- tokens: bfloat16 [64, 384, 2048], P(('grp', 'fs'), None, 'tp'), parts along dimension 0, may hold values from -24 to 24
- input_gain: float32 [2048], replicated, may hold values from 0.1 to 1.9
- query_weight: bfloat16 [2048, 1024], P('fs', 'tp'), may hold values from -0.125 to 0.125
- key_weight: bfloat16 [2048, 1024], P('fs', 'tp'), may hold values from -0.125 to 0.125
- value_weight: bfloat16 [2048, 1024], P('fs', 'tp'), may hold values from -0.125 to 0.125
- output_gate_matrix: bfloat16 [2048, 1024], P('fs', 'tp'), may hold values from -0.125 to 0.125
- forward_decay: float32 [16], P('tp'), may hold values from -1 to 9
- backward_decay: float32 [16], P('tp'), may hold values from -1 to 9
- merge_weight: bfloat16 [1024, 2048], P('tp', 'fs'), may hold values from -0.375 to 0.375
- middle_gain: float32 [2048], replicated, may hold values from 0.1 to 1.9
- gate_weight: bfloat16 [2048, 5120], P('fs', 'tp'), may hold values from -0.125 to 0.125
- up_weight: bfloat16 [2048, 5120], P('fs', 'tp'), may hold values from -0.125 to 0.125
- down_weight: bfloat16 [5120, 2048], P('tp', 'fs'), may hold values from -0.15625 to 0.15625
Outputs:
- layer_out: bfloat16 [64, 384, 2048], P(('grp', 'fs'), None, 'tp'), parts along dimension 0
There are 2 independent parts, one for each index of `grp`. A program takes and returns all parts, laid end to end along the dimension named above; an argument that names none is the same for every part. Nothing has to cross between parts.
All inputs are finite; a program needn't handle non-finite values.
Results may differ from a plain program's by a relative error of at most 0.019.
Values may be sent and summed in bfloat16 or wider, within the bound.
A program may use at most 64 MiB of HBM per device.

v0:
```python
import jax
import jax.numpy as jnp
from jax import lax
from jax.sharding import PartitionSpec as P

BLOCK = 128
norm_eps = 1e-06
group_eps = 1e-05
rope_base = 10000.0
highest_precision = lax.Precision.HIGHEST


def joined_along(tiles, dim):
    tiles = jnp.moveaxis(tiles, 0, dim)
    lengths = tiles.shape
    return tiles.reshape(*lengths[:dim], lengths[dim] * lengths[dim + 1], *lengths[dim + 2 :])


def copy_for_each(array, axis):
    copies = jnp.broadcast_to(array, (lax.axis_size(axis), *array.shape))
    return lax.all_to_all(copies, axis, split_axis=0, concat_axis=0, tiled=True)


def gathered_copies(array, axis, dim):
    return joined_along(copy_for_each(array, axis), dim)


def sent_together(arrays, axis, dim, along):
    both = jnp.concatenate(arrays, axis=along)
    result, at, gathered = (lax.all_gather(both, axis, axis=dim, tiled=True), 0, [])
    for a in arrays:
        gathered.append(lax.slice_in_dim(result, at, at + a.shape[along], axis=along))
        at += a.shape[along]
    return tuple(gathered)


def split_up(array, dim, peers):
    lengths = array.shape
    tiles = array.reshape(*lengths[:dim], peers, lengths[dim] // peers, *lengths[dim + 1 :])
    return jnp.moveaxis(tiles, dim, 0)


def summed_on_arrival(array, axis, dim):
    peers = lax.axis_size(axis)
    tiles = lax.all_to_all(split_up(array, dim, peers), axis, 0, 0, tiled=True)
    return jnp.sum(tiles.astype(jnp.float32), axis=0)


def rms_scale(values, gain_vector):
    widened = values.astype(jnp.float32)
    scaled = widened * lax.rsqrt(jnp.mean(widened * widened, axis=-1, keepdims=True) + norm_eps)
    return (scaled * gain_vector).astype(jnp.bfloat16)


def apply_rotary_heads(values, length):
    half_dim = values.shape[-1] // 2
    inverse = rope_base ** (-jnp.arange(half_dim, dtype=jnp.float32) / half_dim)
    angles = jnp.arange(length, dtype=jnp.float32)[:, None] * inverse[None, :]
    cosine = jnp.cos(angles)[:, None, :]
    sine_part = jnp.sin(angles)[:, None, :]
    lower_half = values[..., :half_dim]
    upper_half = values[..., half_dim:]
    return jnp.concatenate(
        [
            lower_half * cosine - upper_half * sine_part,
            upper_half * cosine + lower_half * sine_part,
        ],
        axis=-1,
    )


def carry_states(key_blocks, value_blocks, weighting, log_rates, block_size, backward):
    block_terms = jnp.einsum(
        "sbmhd,sbmhe->bshde",
        key_blocks * weighting[None, None, :, :, None],
        value_blocks,
        precision=highest_precision,
    )
    factor = jnp.exp(log_rates * block_size)[None, :, None, None]

    def advance(running, addend):
        return (running * factor + addend, running)

    initial = jnp.zeros(block_terms.shape[1:], jnp.float32)
    return lax.scan(advance, initial, block_terms, reverse=backward)[1]


def retain_blocks(
    query_rows, key_rows, value_rows, gate_rows, forward_decay, backward_decay, seq_count, length
):
    head_count = forward_decay.shape[0]
    head_dim = query_rows.shape[1] // head_count
    block_size = BLOCK
    block_count = length // block_size

    def split_heads(rows_in):
        return rows_in.astype(jnp.float32).reshape(seq_count, length, head_count, head_dim)

    def blocked(tensor):
        return tensor.reshape(seq_count, block_count, block_size, head_count, head_dim)

    queries = blocked(apply_rotary_heads(split_heads(query_rows), length))
    key_heads = blocked(apply_rotary_heads(split_heads(key_rows), length) * head_dim ** (-0.5))
    valued = blocked(split_heads(value_rows))
    rate_ahead = jax.nn.log_sigmoid(forward_decay)
    rate_behind = jax.nn.log_sigmoid(backward_decay)
    position = jnp.arange(block_size, dtype=jnp.float32)
    offset = position[:, None] - position[None, :]
    inside = jnp.where(
        offset[None] >= 0,
        jnp.exp(rate_ahead[:, None, None] * jnp.maximum(offset, 0.0)[None]),
        jnp.exp(rate_behind[:, None, None] * jnp.maximum(-offset, 0.0)[None]),
    )
    attention_scores = (
        jnp.einsum("sbchd,sbmhd->sbhcm", queries, key_heads, precision=highest_precision)
        * inside[None, None]
    )
    result = jnp.einsum("sbhcm,sbmhd->sbchd", attention_scores, valued, precision=highest_precision)
    column = position[:, None]
    key_ahead = jnp.exp(rate_ahead[None, :] * (block_size - 1 - column))
    query_ahead = jnp.exp(rate_ahead[None, :] * (column + 1))
    key_behind = jnp.exp(rate_behind[None, :] * column)
    query_behind = jnp.exp(rate_behind[None, :] * (block_size - column))
    from_before = carry_states(key_heads, valued, key_ahead, rate_ahead, block_size, False)
    from_after = carry_states(key_heads, valued, key_behind, rate_behind, block_size, True)
    result = (
        result
        + jnp.einsum("sbchd,bshde->sbche", queries, from_before, precision=highest_precision)
        * query_ahead[None, None, :, :, None]
    )
    result = (
        result
        + jnp.einsum("sbchd,bshde->sbche", queries, from_after, precision=highest_precision)
        * query_behind[None, None, :, :, None]
    )
    result = result.reshape(seq_count, length, head_count, head_dim)
    center = jnp.mean(result, axis=-1, keepdims=True)
    spread = jnp.mean(jnp.square(result - center), axis=-1, keepdims=True)
    normalized = (result - center) * lax.rsqrt(spread + group_eps)
    gated = jax.nn.silu(split_heads(gate_rows)) * normalized
    return gated.reshape(seq_count * length, head_count * head_dim).astype(jnp.bfloat16)


def accumulate(pieces, source):
    return tuple(
        (
            jnp.dot(source, weight_piece, preferred_element_type=jnp.float32)
            for weight_piece in pieces
        )
    )


def on_device(
    tokens,
    input_gain,
    query_weight,
    key_weight,
    value_weight,
    output_gate_matrix,
    forward_decay,
    backward_decay,
    merge_weight,
    middle_gain,
    gate_weight,
    up_weight,
    down_weight,
):
    seq_count, length, part_width = tokens.shape
    row_count = seq_count * length
    gathered = gathered_copies(tokens, "tp", 2)
    normed = rms_scale(gathered.reshape(row_count, gathered.shape[2]), input_gain)
    query_sum, key_sum, value_sum, gating_sum = accumulate(
        sent_together((query_weight, key_weight, value_weight, output_gate_matrix), "fs", 0, 1),
        normed,
    )
    mixed = retain_blocks(
        query_sum.astype(jnp.bfloat16),
        key_sum.astype(jnp.bfloat16),
        value_sum.astype(jnp.bfloat16),
        gating_sum.astype(jnp.bfloat16),
        forward_decay,
        backward_decay,
        seq_count,
        length,
    )
    merge_term = jnp.dot(
        mixed,
        lax.all_gather(merge_weight, "fs", axis=1, tiled=True),
        preferred_element_type=jnp.float32,
    )
    merged = summed_on_arrival(merge_term.astype(jnp.bfloat16), "tp", 1)
    middle = (tokens.reshape(row_count, part_width).astype(jnp.float32) + merged).astype(
        jnp.bfloat16
    )
    gathered_mid = gathered_copies(middle, "tp", 1)
    normed_mid = rms_scale(gathered_mid, middle_gain)
    gate_full, up_full = sent_together((gate_weight, up_weight), "fs", 0, 1)
    gate_act = jnp.dot(normed_mid, gate_full, preferred_element_type=jnp.float32)
    up_act = jnp.dot(normed_mid, up_full, preferred_element_type=jnp.float32)
    hidden = (jax.nn.silu(gate_act) * up_act).astype(jnp.bfloat16)
    down_term = jnp.dot(
        hidden,
        lax.all_gather(down_weight, "fs", axis=1, tiled=True),
        preferred_element_type=jnp.float32,
    )
    summed = summed_on_arrival(down_term.astype(jnp.bfloat16), "tp", 1)
    layer_out = (middle.astype(jnp.float32) + summed).astype(jnp.bfloat16)
    return layer_out.reshape(seq_count, length, part_width)


def solution(mesh):
    placed = (
        P(("grp", "fs"), None, "tp"),
        P(),
        P("fs", "tp"),
        P("fs", "tp"),
        P("fs", "tp"),
        P("fs", "tp"),
        P("tp"),
        P("tp"),
        P("tp", "fs"),
        P(),
        P("fs", "tp"),
        P("fs", "tp"),
        P("tp", "fs"),
    )
    return jax.shard_map(
        on_device,
        mesh=mesh,
        in_specs=placed,
        out_specs=P(("grp", "fs"), None, "tp"),
        check_vma=False,
    )
```

profile of v0, /device:TPU:33, one launch (start us, length us, event | category | flops | bytes accessed | tf_op | source)
XLA Modules:
  0.0 478.5 jit_solution(4488102892256830335)
XLA Ops:
  6.6 1.4 pad_maximum_fusion.2
  8.0 0.1 all-gather.4.cloned.1.call-update
  8.0 0.1 all-gather.6.cloned.1.call-start
  8.1 1.6 pad_maximum_fusion.1
  9.7 0.1 all-gather.6.cloned.1.call-update
  9.8 1.1 copy.41
  10.9 1.3 broadcast_in_dim.28
  12.1 45.1 %all-to-all-start = ((bf16[8,1,384,256]{2,3,1,0:T(8,128)(2,1)}), bf16[8,1,384,256]{2,3,1,0:T(8,128)(2,1)S(1)}, u32[]{:S(2)}, u32[]{:S(2)}) async-start(bf16[8,1,384,256]{2,3,1,0:T(8,128)(2,1)} %broadcast_in_dim.28), calls=%async_computation | async-start | bytes 3145728 | tf_op jit(solution)/shard_map/all_to_all | solution.py:21
  57.2 0.7 all-gather.8.cloned.1.call-update
  58.1 0.1 multiply_exponential_fusion
  58.2 0.1 multiply_exponential_fusion.1
  58.3 0.3 fusion.47
  58.6 0.1 exponential_select_fusion
  58.7 51.9 %all_gather.13 = bf16[128,2048]{0,1:T(8,128)(2,1)} all-gather(bf16[128,64]{0,1:T(8,128)(2,1)S(1)} %copy-done.2), channel_id=1, replica_groups=mesh['grp'=2,'fs'=32,'tp'=8] {'fs'}, dimensions={1}, use_global_device_ids=true | all-gather | bytes 540672 | tf_op jit(solution)/shard_map/all_gather | solution.py:188
  110.6 0.0 all-to-all-done
  110.6 0.4 multiply_reduce_fusion.1
  111.1 0.2 bitcast_convert_fusion
  111.3 0.5 copy-done.3
  111.8 0.4 fusion.3
  112.1 38.8 %all-gather.4.cloned.1.call-done = bf16[2048,512]{1,0:T(8,128)(2,1)} async-done(((bf16[64,512]{1,0:T(8,128)(2,1)}), bf16[2048,512]{1,0:T(8,128)(2,1)}) %all-gather.4.cloned.1.call-update) | async-done | bytes 2097168 | tf_op jit(solution)/shard_map/all_gather | solution.py:30
  150.9 1.5 convolution_convert_fusion.3
  152.5 1.5 convolution_convert_fusion.2
  154.1 0.1 multiply_subtract_fusion.1
  154.2 1.7 convolution_convert_fusion.4
  155.9 0.1 reshape.440
  156.0 0.1 copy.47
  156.2 0.3 convolution_bitcast_fusion.4
  156.5 0.3 while.30
  156.5 0.1 bitcast_add_fusion.6
  156.6 0.1 bitcast_add_fusion.6
  156.7 0.1 bitcast_add_fusion.6
  156.8 0.1 reshape.425
  156.9 0.3 convolution_bitcast_fusion.3
  157.2 0.3 while.31
  157.2 0.1 bitcast_add_fusion.7
  157.3 0.1 bitcast_add_fusion.7
  157.4 0.1 bitcast_add_fusion.7
  157.5 0.8 convolution_multiply_fusion
  158.3 0.5 fusion.16
  158.8 0.5 fusion.17
  159.3 0.5 fusion.56
  159.8 0.2 copy.65
  160.0 0.9 reshape.439
  161.1 0.1 copy.59
  161.2 0.1 copy.58
  161.3 3.2 convolution_convert_fusion.1
  164.5 0.1 copy.82
  164.6 0.0 copy-start
  164.6 46.3 %all_to_all.20 = bf16[8,384,256]{2,1,0:T(8,128)(2,1)S(1)} all-to-all(bf16[8,384,256]{2,1,0:T(8,128)(2,1)S(1)} %bitcast.140), channel_id=1, replica_groups=mesh['grp'=2,'fs'=32,'tp'=8] {'tp'}, dimensions={0} | all-to-all | bytes 3145728 | tf_op jit(solution)/shard_map/all_to_all | solution.py:45
  210.9 0.2 convert_reduce_fusion.1
  211.2 0.2 copy.61
  211.3 0.1 broadcast_in_dim.33
  211.5 0.0 copy-start.4
  211.5 24.2 %all_to_all.21 = bf16[8,384,256]{1,2,0:T(8,128)(2,1)S(1)} all-to-all(bf16[8,384,256]{1,2,0:T(8,128)(2,1)S(1)} %broadcast_in_dim.33), channel_id=1, replica_groups=mesh['grp'=2,'fs'=32,'tp'=8] {'tp'}, dimensions={0} | all-to-all | bytes 3145728 | tf_op jit(solution)/shard_map/all_to_all | solution.py:21
  235.7 0.4 multiply_reduce_fusion
  236.1 0.4 fusion.1
  236.5 52.4 %all-gather.6.cloned.1.call-done = bf16[2048,1280]{1,0:T(8,128)(2,1)} async-done(((bf16[64,1280]{1,0:T(8,128)(2,1)}), bf16[2048,1280]{1,0:T(8,128)(2,1)}) %all-gather.6.cloned.1.call-update) | async-done | bytes 5242896 | tf_op jit(solution)/shard_map/all_gather | solution.py:30
  288.9 3.2 fusion.6
  292.1 126.9 %all-gather.8.cloned.1.call-done = bf16[640,2048]{0,1:T(8,128)(2,1)} async-done(((bf16[640,64]{0,1:T(8,128)(2,1)}), bf16[640,2048]{0,1:T(8,128)(2,1)}) %all-gather.8.cloned.1.call-update) | async-done | bytes 2621456 | tf_op jit(solution)/shard_map/all_gather | solution.py:203
  419.0 6.2 %convolution_convert_fusion = bf16[384,2048]{1,0:T(8,128)(2,1)S(1)} fusion(bf16[640,2048]{0,1:T(8,128)(2,1)} %all-gather.8.cloned.1.call-done, bf16[384,2048]{0,1:T(8,128)(2,1)} %copy-done.1, bf16[2048,1280]{1,0:T(8,128)(2,1)} %all-gather.6.cloned.1.call-done, f32[384,640]{1,0:T(8,128)S(1)} %fusion.6), kind=kOutput, calls=%fused_computation.14 | convolution fusion | flops 2015526912 | bytes 9371648 | tf_op jit(solution)/shard_map/dot_general | solution.py:201
  425.1 0.1 copy.81
  425.3 45.7 %all_to_all.22 = bf16[8,384,256]{2,1,0:T(8,128)(2,1)S(1)} all-to-all(bf16[8,384,256]{2,1,0:T(8,128)(2,1)S(1)} %bitcast.141), channel_id=1, replica_groups=mesh['grp'=2,'fs'=32,'tp'=8] {'tp'}, dimensions={0} | all-to-all | bytes 3145728 | tf_op jit(solution)/shard_map/all_to_all | solution.py:45
  471.0 0.2 convert_reduce_fusion
  471.2 0.8 fusion.26
  (44 shorter events, 0.5 us)
Async XLA Ops:
  6.5 144.4 %all-gather.4.cloned.1.call-start = ((), (), s32[]{:S(2)}) async-start(), calls=%async_computation.4 | async-start | bytes 2162688 | tf_op jit(solution)/shard_map/all_gather | solution.py:30
  8.0 280.9 %all-gather.6.cloned.1.call-start = ((), (), s32[]{:S(2)}) async-start(), calls=%async_computation.5 | async-start | bytes 5406720 | tf_op jit(solution)/shard_map/all_gather | solution.py:30
  12.1 46.0 %copy-start.5 = (f32[2]{0:T(128)S(1)}, f32[2]{0:T(128)}, u32[]{:S(2)}) copy-start(f32[2]{0:T(128)} %param.24) | copy-start | bytes 28
  12.1 46.0 %copy-start.6 = (f32[2]{0:T(128)S(1)}, f32[2]{0:T(128)}, u32[]{:S(2)}) copy-start(f32[2]{0:T(128)} %param.23) | copy-start | bytes 28
  12.1 46.5 %copy-start.2 = (bf16[128,64]{0,1:T(8,128)(2,1)S(1)}, bf16[128,64]{0,1:T(8,128)(2,1)}, u32[]{:S(2)}) copy-start(bf16[128,64]{0,1:T(8,128)(2,1)} %param.25) | copy-start | bytes 49156
  12.1 98.5 %all-to-all-start = ((bf16[8,1,384,256]{2,3,1,0:T(8,128)(2,1)}), bf16[8,1,384,256]{2,3,1,0:T(8,128)(2,1)S(1)}, u32[]{:S(2)}, u32[]{:S(2)}) async-start(bf16[8,1,384,256]{2,3,1,0:T(8,128)(2,1)} %broadcast_in_dim.28), calls=%async_computation | async-start | bytes 3145728 | tf_op jit(solution)/shard_map/all_to_all | solution.py:21
  57.2 361.8 %all-gather.8.cloned.1.call-start = ((), (), s32[]{:S(2)}) async-start(), calls=%async_computation.6 | async-start | bytes 2703360 | tf_op jit(solution)/shard_map/all_gather | solution.py:203
  111.1 0.7 copy-start.3
  164.6 46.5 %copy-start = (bf16[1,384,256]{2,1,0:T(8,128)(2,1)S(1)}, bf16[1,384,256]{2,1,0:T(8,128)(2,1)}, u32[]{:S(2)}) copy-start(bf16[1,384,256]{2,1,0:T(8,128)(2,1)} %param.17) | copy-start | bytes 589828
  211.5 24.6 %copy-start.4 = (f32[2048]{0:T(1024)S(1)}, f32[2048]{0:T(1024)}, u32[]{:S(2)}) copy-start(f32[2048]{0:T(1024)} %param.26) | copy-start | bytes 24580
  236.5 55.6 %copy-start.1 = (bf16[384,2048]{0,1:T(8,128)(2,1)}, bf16[384,2048]{0,1:T(8,128)(2,1)S(1)}, u32[]{:S(2)}) copy-start(bf16[384,2048]{0,1:T(8,128)(2,1)S(1)} %fusion.1) | copy-start | bytes 4718596
Sparse Core Ops, SparseCore 0:
  9.4 141.4 all-gather.3
  153.0 135.8 all-gather.5
  291.0 127.9 all-gather.7
where the time goes:
time: 479 us
  waiting for transfers between devices  219 us (46%)
  blocking collectives  168 us (35%)
  starting transfers between devices  45.1 us (9%)
  matrix products  20.1 us (4%)
  between operations  13.6 us (3%)
  other arithmetic  7.42 us (2%)
  local copies, waits for them, and re-layouts  5.26 us (1%)
    all_gather x1, waiting for transfers between devices, on_device(): lax.all_gather(down_weight, 'fs', axis=1, tiled=True)  127 us
    all_to_all x2, blocking collectives, summed_on_arrival(): tiles = lax.all_to_all(split_up(array, dim, peers), axis, 0, 0, tiled=True)  92 us
    all_gather x2, waiting for transfers between devices, sent_together(): lax.all_gather(both, axis, axis=dim, tiled=True)  91.2 us
    all_gather x1, blocking collectives, on_device(): lax.all_gather(merge_weight, 'fs', axis=1, tiled=True)  51.9 us
    all_to_all x1, starting transfers between devices, copy_for_each(): return lax.all_to_all(copies, axis, split_axis=0, concat_axis=0, tiled=True)  45.1 us
    all_to_all x1, blocking collectives, copy_for_each(): return lax.all_to_all(copies, axis, split_axis=0, concat_axis=0, tiled=True)  24.2 us
  transfers between devices with their start and end apart: 4, of which 3 were waited for; matrix products, arithmetic and copies ran while one was open for 5% of the time, Pallas kernels for 0%

commit v1 on v0

--- a/solution.py
+++ b/solution.py
@@ -200,7 +200,9 @@
     hidden = (jax.nn.silu(gate_act) * up_act).astype(jnp.bfloat16)
     down_term = jnp.dot(
         hidden,
-        lax.all_gather(down_weight, "fs", axis=1, tiled=True),
+        jnp.concatenate(
+            lax.all_to_all(jnp.stack([down_weight] * lax.axis_size("fs")), "fs", 0, 0), axis=1
+        ),
         preferred_element_type=jnp.float32,
     )
     summed = summed_on_arrival(down_term.astype(jnp.bfloat16), "tp", 1)

time: 479 us -> 612 us (1.28)
  waiting for transfers between devices: 219 us -> 347 us
  starting transfers between devices: 45.1 us -> 58.6 us
  blocking collectives: 168 us -> 156 us
    all_gather x2, waiting for transfers between devices: 91.2 us -> 347 us  [sent_together(): lax.all_gather(both, axis, axis=dim, tiled=True)]
    all_gather x1 -> x0, waiting for transfers between devices: 127 us -> none  [on_device(): lax.all_gather(down_weight, 'fs', axis=1, tiled=True)]
    all_to_all x0 -> x1, starting transfers between devices: none -> 13.3 us  [on_device(): lax.all_to_all(jnp.stack([down_weight] * lax.axis_size('fs')), 'fs', 0, 0)]
    all_to_all x2, blocking collectives: 92 us -> 80.3 us  [summed_on_arrival(): tiles = lax.all_to_all(split_up(array, dim, peers), axis, 0, 0, tiled=True)]
  transfers between devices with their start and end apart: 4 -> 4, of which waited for: 3 -> 2; matrix products, arithmetic and copies ran while one was open for 5% -> 2% of each run, Pallas kernels for 0% -> 0%
where the time goes in v1:
time: 612 us; the launch traced here: 611 us
  waiting for transfers between devices  347 us (57%)
  blocking collectives  156 us (25%)
  starting transfers between devices  58.6 us (10%)
  matrix products  20.6 us (3%)
  between operations  13.9 us (2%)
  local copies, waits for them, and re-layouts  7.88 us (1%)
  other arithmetic  7.65 us (1%)
    all_gather x2, waiting for transfers between devices, sent_together(): lax.all_gather(both, axis, axis=dim, tiled=True)  347 us
    all_to_all x2, blocking collectives, summed_on_arrival(): tiles = lax.all_to_all(split_up(array, dim, peers), axis, 0, 0, tiled=True)  80.3 us
    all_gather x1, blocking collectives, on_device(): lax.all_gather(merge_weight, 'fs', axis=1, tiled=True)  51.5 us
    all_to_all x1, starting transfers between devices, copy_for_each(): return lax.all_to_all(copies, axis, split_axis=0, concat_axis=0, tiled=True)  45.1 us
    all_to_all x1, blocking collectives, copy_for_each(): return lax.all_to_all(copies, axis, split_axis=0, concat_axis=0, tiled=True)  24.1 us
    all_to_all x1, starting transfers between devices, on_device(): lax.all_to_all(jnp.stack([down_weight] * lax.axis_size('fs')), 'fs', 0, 0)  13.3 us
  transfers between devices with their start and end apart: 4, of which 2 were waited for; matrix products, arithmetic and copies ran while one was open for 2% of the time, Pallas kernels for 0%

profile of v1, /device:TPU:33, one launch (start us, length us, event | category | flops | bytes accessed | tf_op | source)
XLA Modules:
  0.0 611.3 jit_solution(9799533186737019383)
XLA Ops:
  6.6 1.4 pad_maximum_fusion.2
  8.0 0.1 all-gather.3.cloned.1.call-update
  8.0 1.1 copy.42
  9.1 0.0 copy-start.7
  9.1 0.0 copy-start.8
  9.1 1.3 broadcast_in_dim.28
  10.4 45.1 %all-to-all-start = ((bf16[8,1,384,256]{2,3,1,0:T(8,128)(2,1)}), bf16[8,1,384,256]{2,3,1,0:T(8,128)(2,1)S(1)}, u32[]{:S(2)}, u32[]{:S(2)}) async-start(bf16[8,1,384,256]{2,3,1,0:T(8,128)(2,1)} %broadcast_in_dim.28), calls=%async_computation | async-start | bytes 3145728 | tf_op jit(solution)/shard_map/all_to_all | solution.py:21
  55.7 0.1 multiply_exponential_fusion
  55.7 0.1 multiply_exponential_fusion.1
  55.8 0.3 fusion.47
  56.1 0.1 exponential_select_fusion
  56.2 51.5 %all_gather.10 = bf16[128,2048]{0,1:T(8,128)(2,1)} all-gather(bf16[128,64]{0,1:T(8,128)(2,1)S(1)} %copy-done.4), channel_id=1, replica_groups=mesh['grp'=2,'fs'=32,'tp'=8] {'fs'}, dimensions={1}, use_global_device_ids=true | all-gather | bytes 540672 | tf_op jit(solution)/shard_map/all_gather | solution.py:188
  107.7 0.4 multiply_reduce_fusion.1
  108.2 0.2 bitcast_convert_fusion
  108.4 0.5 copy-done.5
  108.9 0.4 fusion.3
  109.2 41.9 %all-gather.3.cloned.1.call-done = bf16[2048,512]{1,0:T(8,128)(2,1)} async-done(((bf16[64,512]{1,0:T(8,128)(2,1)}), bf16[2048,512]{1,0:T(8,128)(2,1)}) %all-gather.3.cloned.1.call-update) | async-done | bytes 2097168 | tf_op jit(solution)/shard_map/all_gather | solution.py:30
  151.2 1.7 convolution_convert_fusion.4
  152.8 0.1 reshape.450
  153.0 0.1 copy.48
  153.1 1.5 convolution_convert_fusion.3
  154.7 1.5 convolution_convert_fusion.2
  156.2 0.1 multiply_subtract_fusion.1
  156.4 0.3 convolution_bitcast_fusion.3
  156.7 0.3 while.31
  156.8 0.1 bitcast_add_fusion.7
  156.8 0.1 bitcast_add_fusion.7
  156.9 0.1 bitcast_add_fusion.7
  157.0 0.1 reshape.433
  157.1 0.3 convolution_bitcast_fusion.4
  157.4 0.3 while.30
  157.5 0.1 bitcast_add_fusion.6
  157.6 0.1 bitcast_add_fusion.6
  157.7 0.1 bitcast_add_fusion.6
  157.7 0.8 convolution_multiply_fusion
  158.5 0.5 fusion.17
  159.0 0.5 fusion.16
  159.5 0.5 fusion.56
  160.1 0.2 copy.66
  160.4 0.1 copy.60
  160.5 0.9 reshape.449
  161.4 0.8 copy.59
  162.2 3.2 convolution_convert_fusion.1
  165.5 0.1 copy.83
  165.6 0.0 copy-start
  165.6 45.7 %all_to_all.25 = bf16[8,384,256]{2,1,0:T(8,128)(2,1)S(1)} all-to-all(bf16[8,384,256]{2,1,0:T(8,128)(2,1)S(1)} %bitcast.143), channel_id=1, replica_groups=mesh['grp'=2,'fs'=32,'tp'=8] {'tp'}, dimensions={0} | all-to-all | bytes 3145728 | tf_op jit(solution)/shard_map/all_to_all | solution.py:45
  211.3 0.2 convert_reduce_fusion.1
  211.6 0.2 copy.62
  211.8 0.1 broadcast_in_dim.33
  211.9 24.1 %all_to_all.26 = bf16[8,384,256]{1,2,0:T(8,128)(2,1)S(1)} all-to-all(bf16[8,384,256]{1,2,0:T(8,128)(2,1)S(1)} %broadcast_in_dim.33), channel_id=1, replica_groups=mesh['grp'=2,'fs'=32,'tp'=8] {'tp'}, dimensions={0} | all-to-all | bytes 3145728 | tf_op jit(solution)/shard_map/all_to_all | solution.py:21
  236.0 1.9 stack.2
  237.9 13.3 %all-to-all-start.3 = ((bf16[32,640,64]{1,2,0:T(8,128)(2,1)}), bf16[32,640,64]{1,2,0:T(8,128)(2,1)}, u32[]{:S(2)}, u32[]{:S(2)}) async-start(bf16[32,640,64]{1,2,0:T(8,128)(2,1)} %stack.2), calls=%async_computation.3 | async-start | bytes 5242880 | tf_op jit(solution)/shard_map/all_to_all | solution.py:204
  251.2 0.2 all-gather.5.cloned.1.call-start
  251.5 0.7 pad_maximum_fusion.1
  252.2 0.1 all-gather.5.cloned.1.call-update
  252.2 0.4 multiply_reduce_fusion
  252.7 1.6 fusion.1
  254.3 304.6 %all-gather.5.cloned.1.call-done = bf16[2048,1280]{1,0:T(8,128)(2,1)} async-done(((bf16[64,1280]{1,0:T(8,128)(2,1)}), bf16[2048,1280]{1,0:T(8,128)(2,1)}) %all-gather.5.cloned.1.call-update) | async-done | bytes 5242896 | tf_op jit(solution)/shard_map/all_gather | solution.py:30
  558.9 3.6 fusion.6
  562.5 6.2 %convolution_convert_fusion = bf16[384,2048]{1,0:T(8,128)(2,1)S(1)} fusion(bf16[640,2048]{0,1:T(8,128)(2,1)} %bitcast.31, bf16[384,2048]{0,1:T(8,128)(2,1)} %fusion.1, bf16[2048,1280]{1,0:T(8,128)(2,1)} %all-gather.5.cloned.1.call-done, f32[384,640]{1,0:T(8,128)S(1)} %fusion.6), kind=kOutput, calls=%fused_computation.14 | convolution fusion | flops 2015526912 | bytes 9371648 | tf_op jit(solution)/shard_map/dot_general | solution.py:201
  568.7 0.1 copy.82
  568.8 34.6 %all_to_all.27 = bf16[8,384,256]{2,1,0:T(8,128)(2,1)S(1)} all-to-all(bf16[8,384,256]{2,1,0:T(8,128)(2,1)S(1)} %bitcast.144), channel_id=1, replica_groups=mesh['grp'=2,'fs'=32,'tp'=8] {'tp'}, dimensions={0} | all-to-all | bytes 3145728 | tf_op jit(solution)/shard_map/all_to_all | solution.py:45
  603.4 0.2 convert_reduce_fusion
  603.7 0.7 fusion.26
  (48 shorter events, 0.5 us)
Async XLA Ops:
  6.5 144.6 %all-gather.3.cloned.1.call-start = ((), (), s32[]{:S(2)}) async-start(), calls=%async_computation.5 | async-start | bytes 2162688 | tf_op jit(solution)/shard_map/all_gather | solution.py:30
  9.1 46.5 %copy-start.7 = (f32[2]{0:T(128)S(1)}, f32[2]{0:T(128)}, u32[]{:S(2)}) copy-start(f32[2]{0:T(128)} %param.24) | copy-start | bytes 28
  9.1 46.5 %copy-start.8 = (f32[2]{0:T(128)S(1)}, f32[2]{0:T(128)}, u32[]{:S(2)}) copy-start(f32[2]{0:T(128)} %param.23) | copy-start | bytes 28
  10.4 45.8 %copy-start.4 = (bf16[128,64]{0,1:T(8,128)(2,1)S(1)}, bf16[128,64]{0,1:T(8,128)(2,1)}, u32[]{:S(2)}) copy-start(bf16[128,64]{0,1:T(8,128)(2,1)} %param.25) | copy-start | bytes 49156
  10.4 97.3 %all-to-all-start = ((bf16[8,1,384,256]{2,3,1,0:T(8,128)(2,1)}), bf16[8,1,384,256]{2,3,1,0:T(8,128)(2,1)S(1)}, u32[]{:S(2)}, u32[]{:S(2)}) async-start(bf16[8,1,384,256]{2,3,1,0:T(8,128)(2,1)} %broadcast_in_dim.28), calls=%async_computation | async-start | bytes 3145728 | tf_op jit(solution)/shard_map/all_to_all | solution.py:21
  108.2 0.7 copy-start.5
  165.6 46.0 %copy-start = (bf16[1,384,256]{2,1,0:T(8,128)(2,1)S(1)}, bf16[1,384,256]{2,1,0:T(8,128)(2,1)}, u32[]{:S(2)}) copy-start(bf16[1,384,256]{2,1,0:T(8,128)(2,1)} %param.17) | copy-start | bytes 589828
  211.8 24.3 %copy-start.3 = (bf16[640,64]{0,1:T(8,128)(2,1)S(1)}, bf16[640,64]{0,1:T(8,128)(2,1)}, u32[]{:S(2)}) copy-start(bf16[640,64]{0,1:T(8,128)(2,1)} %param.29) | copy-start | bytes 245764
  237.9 13.6 %copy-start.1 = (bf16[64,640]{1,0:T(8,128)(2,1)S(1)}, bf16[64,640]{1,0:T(8,128)(2,1)}, u32[]{:S(2)}) copy-start(bf16[64,640]{1,0:T(8,128)(2,1)} %param.28) | copy-start | bytes 245764
  237.9 13.6 %copy-start.2 = (bf16[64,640]{1,0:T(8,128)(2,1)S(1)}, bf16[64,640]{1,0:T(8,128)(2,1)}, u32[]{:S(2)}) copy-start(bf16[64,640]{1,0:T(8,128)(2,1)} %param.27) | copy-start | bytes 245764
  237.9 14.7 %copy-start.6 = (f32[2048]{0:T(1024)S(1)}, f32[2048]{0:T(1024)}, u32[]{:S(2)}) copy-start(f32[2048]{0:T(1024)} %param.26) | copy-start | bytes 24580
  237.9 324.6 %all-to-all-start.3 = ((bf16[32,640,64]{1,2,0:T(8,128)(2,1)}), bf16[32,640,64]{1,2,0:T(8,128)(2,1)}, u32[]{:S(2)}, u32[]{:S(2)}) async-start(bf16[32,640,64]{1,2,0:T(8,128)(2,1)} %stack.2), calls=%async_computation.3 | async-start | bytes 5242880 | tf_op jit(solution)/shard_map/all_to_all | solution.py:204
  251.2 307.6 %all-gather.5.cloned.1.call-start = ((), (), s32[]{:S(2)}) async-start(), calls=%async_computation.6 | async-start | bytes 5406720 | tf_op jit(solution)/shard_map/all_gather | solution.py:30
Sparse Core Ops, SparseCore 0:
  9.4 141.6 all-gather.2
  254.2 304.6 all-gather.4
